TPU v7x, 32 devices: a whole 2x2x4 slice. The times are simulated.
32 devices in a mesh: sp: 8 (over z, y), tp: 4 (over x, core).
Axes of the slice: x: 2, y: 2, z: 4, core: 2. Of those that a mesh axis runs over, the one named last changes fastest.
Arguments:
- tokens: bfloat16 [4096, 2048], P('sp', 'tp'), may hold values from -400 to 400
- norm_gain: float32 [2048], replicated, may hold values from 0.1 to 1.9
- query_weight: bfloat16 [2048, 1024], P(None, 'tp'), may hold values from -0.37306796 to 0.37306796
- key_weight: bfloat16 [2048, 1024], P(None, 'tp'), may hold values from -0.2625825 to 0.2625825
- value_weight: bfloat16 [2048, 1024], P(None, 'tp'), may hold values from -0.125 to 0.125
- outer_gate_weight: bfloat16 [2048, 1024], P(None, 'tp'), may hold values from -0.125 to 0.125
- inner_gate_weight: bfloat16 [2048, 1024], P(None, 'tp'), may hold values from -0.125 to 0.125
- conv_input_weight: bfloat16 [2048, 1024], P(None, 'tp'), may hold values from -0.125 to 0.125
- conv_taps: float32 [3, 1024], P(None, 'tp'), may hold values from -3.5 to 3.5
- lambdas: float32 [8], P('tp'), may hold values from 0.3 to 0.8
- head_gain: float32 [128], replicated, may hold values from 0.1 to 1.9
- attn_out_weight: bfloat16 [1024, 2048], P(None, 'tp'), may hold values from -0.125 to 0.125
- conv_out_weight: bfloat16 [1024, 2048], P(None, 'tp'), may hold values from -0.125 to 0.125
Outputs:
- mixed_out: bfloat16 [4096, 2048], P('sp', 'tp')
- log_totals: float32 [8, 2, 4096], P('tp', None, 'sp')
All inputs are finite; a program needn't handle non-finite values.
Results may differ from a plain program's by a relative error of at most 0.014.
The roundings to bfloat16 on the way count: a program that leaves them out, or rounds other values in their place, can miss the bound.
Values may be sent and summed in bfloat16 or wider, within the bound.
A program may use at most 128 MiB of HBM per device.

v0:
```python
import math
import jax
import jax.numpy as jnp
from jax import lax
from jax.sharding import PartitionSpec as P

NORM_EPS = 1e-06
HEAD_EPS = 1e-05
ROPE_BASE = 500000.0
MASKED = -1e30
HEAD_SCALE = 0.8


def shifted(block, axis, distance):
    devices = range(lax.axis_size(axis))
    route = [(i - distance, i) for i in devices if i - distance in devices]
    return lax.ppermute(block, axis, route)


def rotate(field_in, positions):
    half_dim = field_in.shape[-1] // 2
    frequency = ROPE_BASE ** (-jnp.arange(half_dim, dtype=jnp.float32) * 2.0 / field_in.shape[-1])
    angles = positions[:, None] * frequency[None, :]
    cosine = jnp.cos(angles)[:, None, None, :]
    sine_part = jnp.sin(angles)[:, None, None, :]
    first_half = field_in[..., :half_dim]
    second_half = field_in[..., half_dim:]
    return jnp.concatenate(
        [
            first_half * cosine - second_half * sine_part,
            second_half * cosine + first_half * sine_part,
        ],
        axis=-1,
    )


def add_products(block_in, norm_gain, weights):
    floats = block_in.astype(jnp.float32)
    scaled = (floats * norm_gain[None, :]).astype(jnp.bfloat16)
    products = tuple(
        (jnp.dot(scaled, weight, preferred_element_type=jnp.float32) for weight in weights)
    )
    return (jnp.sum(floats * floats, axis=1, keepdims=True),) + products


def over_shards(step_fn, running, arrays, anchor, local_rows):
    shard_count = arrays[0].shape[0] // local_rows
    group_size = math.gcd(shard_count, max(1, 2048 // local_rows))
    block_rows = group_size * local_rows
    steps_count = shard_count // group_size
    stacked = tuple(
        (member.reshape((steps_count, block_rows) + member.shape[1:]) for member in arrays)
    )

    def scan_step(carried, scan_items):
        members, step_index = scan_items
        return (step_fn(carried, members, anchor + step_index * block_rows), None)

    result, unused = lax.scan(
        scan_step, running, (stacked, jnp.arange(steps_count, dtype=jnp.int32))
    )
    return result


def per_device(
    tokens,
    norm_gain,
    query_weight,
    key_weight,
    value_weight,
    outer_gate_weight,
    inner_gate_weight,
    conv_input_weight,
    conv_taps,
    lambdas,
    head_gain,
    attn_out_weight,
    conv_out_weight,
):
    local_rows = tokens.shape[0]
    local_heads = lambdas.shape[0]
    head_dim = query_weight.shape[1] // (2 * local_heads)
    value_dim = 2 * head_dim
    taps_count = conv_taps.shape[0]
    width_all = norm_gain.shape[0]
    columns_dev = query_weight.shape[1]
    attn_weights = (query_weight, key_weight, value_weight)
    conv_weights = (outer_gate_weight, inner_gate_weight, conv_input_weight)
    squares, query_raw, key_raw, value_raw, outer_raw, inner_raw, signal_raw = add_products(
        lax.all_gather(tokens, "tp", axis=1, tiled=True), norm_gain, attn_weights + conv_weights
    )
    inverse_rms = lax.rsqrt(squares / width_all + NORM_EPS)
    query_pos = lax.axis_index("sp") * local_rows + jnp.arange(local_rows, dtype=jnp.int32)
    positions = query_pos.astype(jnp.float32)
    queries = rotate(
        (inverse_rms * query_raw).reshape(local_rows, local_heads, 2, head_dim), positions
    ).astype(jnp.bfloat16)
    key_rows = rotate(
        (inverse_rms * key_raw).reshape(local_rows, local_heads, 2, head_dim), positions
    ).astype(jnp.bfloat16)
    values = (
        (inverse_rms * value_raw).astype(jnp.bfloat16).reshape(local_rows, local_heads, value_dim)
    )
    outer_gate = (inverse_rms * outer_raw).astype(jnp.bfloat16)
    inner_gate = (inverse_rms * inner_raw).astype(jnp.bfloat16)
    signal = (inverse_rms * signal_raw).astype(jnp.bfloat16)
    conv_in = (inner_gate.astype(jnp.float32) * signal.astype(jnp.float32)).astype(jnp.bfloat16)
    rim_rows = shifted(conv_in[local_rows - (taps_count - 1) :], "sp", 1)
    padded = jnp.concatenate([rim_rows, conv_in], axis=0)
    summed = jnp.zeros((local_rows, columns_dev), jnp.float32)
    for tap_index in range(taps_count):
        summed = summed + conv_taps[tap_index][None, :] * padded[
            tap_index : tap_index + local_rows
        ].astype(jnp.float32)
    conv_out = (outer_gate.astype(jnp.float32) * summed).astype(jnp.bfloat16)
    scale_factor = head_dim ** (-0.5)

    def block_scores(key_block, key_anchor):
        scores = (
            jnp.einsum("qhcd,khcd->hcqk", queries, key_block, preferred_element_type=jnp.float32)
            * scale_factor
        )
        visible = (
            query_pos[:, None]
            >= (key_anchor + jnp.arange(key_block.shape[0], dtype=jnp.int32))[None, :]
        )
        return (jnp.where(visible, scores, MASKED), visible)

    def stats_step(running, members, key_anchor):
        max_before, sum_before = running
        scores, visible = block_scores(members[0], key_anchor)
        max_after = jnp.maximum(max_before, jnp.max(scores, axis=-1))
        exponent = jnp.where(visible, jnp.exp(scores - max_after[..., None]), 0.0)
        return (
            max_after,
            sum_before * jnp.exp(max_before - max_after) + jnp.sum(exponent, axis=-1),
        )

    stats_init = (
        jnp.full((local_heads, 2, local_rows), MASKED, jnp.float32),
        jnp.zeros((local_heads, 2, local_rows), jnp.float32),
    )
    value_init = jnp.zeros((local_rows, local_heads, value_dim), jnp.float32)

    def value_step_with(row_max, row_sum):

        def value_step(running, members, key_anchor):
            scores, visible = block_scores(members[0], key_anchor)
            normalized = jnp.where(
                visible, jnp.exp(scores - row_max[..., None]) / row_sum[..., None], 0.0
            )
            weights = (normalized[:, 0] - lambdas[:, None, None] * normalized[:, 1]).astype(
                jnp.bfloat16
            )
            return running + jnp.einsum(
                "hqk,khv->qhv", weights, members[1], preferred_element_type=jnp.float32
            )

        return value_step

    all_keys, all_values = (
        lax.all_gather(key_rows, "sp", axis=0, tiled=True),
        lax.all_gather(values, "sp", axis=0, tiled=True),
    )
    row_max, row_sum = over_shards(stats_step, stats_init, (all_keys,), 0, local_rows)
    head_mix = over_shards(
        value_step_with(row_max, row_sum), value_init, (all_keys, all_values), 0, local_rows
    )
    log_totals = row_max + jnp.log(row_sum)
    normed = (
        head_mix
        * lax.rsqrt(jnp.mean(head_mix * head_mix, axis=-1, keepdims=True) + HEAD_EPS)
        * head_gain[None, None, :]
        * HEAD_SCALE
    )
    attn_out = normed.astype(jnp.bfloat16).reshape(local_rows, local_heads * value_dim)
    running = jnp.zeros((local_rows, attn_out_weight.shape[1]), jnp.float32)
    running = jnp.dot(
        lax.all_gather(attn_out, "tp", axis=1, tiled=True),
        attn_out_weight,
        preferred_element_type=jnp.float32,
    )
    mixed_out = running + jnp.dot(
        lax.all_gather(conv_out, "tp", axis=1, tiled=True),
        conv_out_weight,
        preferred_element_type=jnp.float32,
    )
    return (mixed_out.astype(jnp.bfloat16), log_totals)


def solution(mesh):
    in_specs = (
        P("sp", "tp"),
        P(),
        P(None, "tp"),
        P(None, "tp"),
        P(None, "tp"),
        P(None, "tp"),
        P(None, "tp"),
        P(None, "tp"),
        P(None, "tp"),
        P("tp"),
        P(),
        P(None, "tp"),
        P(None, "tp"),
    )
    out_specs = (P("sp", "tp"), P("tp", None, "sp"))
    return jax.shard_map(
        per_device, mesh=mesh, in_specs=in_specs, out_specs=out_specs, check_vma=False
    )
```

profile of v0, /device:TPU:0, one launch (start us, length us, event | category | flops | bytes accessed | tf_op | source)
XLA Modules:
  0.0 211.2 jit_solution(9740739602610465239)
XLA Ops:
  7.2 0.0 copy-start
  7.2 0.0 copy-start.16
  7.2 0.0 all-gather.6.cloned.1.call-start
  7.2 0.7 all-gather.6.cloned.1.call-update
  7.9 0.0 all-gather.10.cloned.1.call-start
  8.0 0.3 multiply_cosine_fusion
  8.3 26.6 %all-gather.6.cloned.1.call-done = bf16[512,2048]{1,0:T(8,128)(2,1)} async-done(((bf16[512,512]{1,0:T(8,128)(2,1)}), bf16[512,2048]{1,0:T(8,128)(2,1)}) %all-gather.6.cloned.1.call-update) | async-done | bytes 2097168 | tf_op jit(solution)/shard_map/all_gather | solution.py:90
  34.9 2.2 %fusion.32 = f32[512]{0:T(512)S(1)} fusion(bf16[512,2048]{1,0:T(8,128)(2,1)} %all-gather.6.cloned.1.call-done), kind=kLoop, calls=%fused_computation.40 | loop fusion | flops 3145216 | bytes 2099200 | tf_op jit(solution)/shard_map/reduce_sum | solution.py:43
  37.1 2.6 %convolution_multiply_fusion.4 = f32[512,256]{0,1:T(8,128)S(1)} fusion(bf16[2048,256]{1,0:T(8,128)(2,1)} %param.20, bf16[512,2048]{1,0:T(8,128)(2,1)} %all-gather.6.cloned.1.call-done, f32[2048]{0:T(1024)} %param.18, f32[512]{0:T(512)S(1)} %add_rsqrt_fusion.1), kind=kOutput, calls=%fused_computation.49 | convolution fusion | flops 540147712 | bytes 3680256 | tf_op jit(solution)/shard_map/dot_general | solution.py:41
  39.8 0.8 convolution_multiply_fusion.3
  40.6 0.2 subtract_convert_fusion
  40.8 0.7 pad_maximum_fusion.1
  41.5 0.0 all-gather.10.cloned.1.call-update
  41.5 0.0 all-gather.8.cloned.1.call-start
  41.6 2.7 %fusion.35 = bf16[512,256]{0,1:T(8,128)(2,1)} fusion(bf16[2048,256]{1,0:T(8,128)(2,1)} %param.21, bf16[512,2048]{1,0:T(8,128)(2,1)S(1)} %copy-done.1, f32[2048]{0:T(1024)} %param.18, f32[512]{0:T(512)S(1)} %add_rsqrt_fusion.1), kind=kOutput, calls=%fused_computation.51 | convolution fusion | flops 540278784 | bytes 3418112 | tf_op jit(solution)/shard_map/dot_general | solution.py:41
  44.3 1.8 copy.21
  46.1 0.0 all-gather.8.cloned.1.call-update
  46.1 0.0 all-gather.12.cloned.1.call-start
  46.2 0.7 pad_maximum_fusion.2
  46.9 45.2 %all-gather.10.cloned.1.call-done = bf16[4096,2,2,64]{0,3,2,1:T(8,128)(2,1)} async-done(((bf16[512,2,2,64]{0,3,2,1:T(8,128)(2,1)}), bf16[4096,2,2,64]{0,3,2,1:T(8,128)(2,1)}) %all-gather.10.cloned.1.call-update) | async-done | bytes 2097168 | tf_op jit(solution)/shard_map/all_gather | solution.py:162
  92.1 1.7 copy.34
  93.8 0.0 copy-start.18
  93.8 18.6 %while.24 = (s32[]{:T(128)}, f32[2,2,512]{2,1,0:T(2,128)S(1)}, f32[2,2,512]{2,1,0:T(2,128)S(1)}, s32[2]{0:T(128)S(1)}, bf16[2,2048,2,2,64]{1,4,3,2,0:T(8,128)(2,...) while((s32[]{:T(128)}, f32[2,2,512]{2,1,0:T(2,128)S(1)}, ...), condition=%wide.region_4.5_spmd.clone, body=%wide.region_1.4_spmd.clone.sunk | while | flops 571486720 | bytes 38138008 | solution.py:59
  93.8 0.6 dynamic_slice.43
  95.1 0.8 broadcast_compare_fusion.4
  95.9 3.0 %fusion.78 = (f32[2,2,512]{2,1,0:T(2,128)S(1)}, f32[2,2,2048,512]{3,2,1,0:T(8,128)S(1)}) fusion(pred[512,2048]{0,1:T(8,128)(4,1)S(1)} %broadcast_compare_fusion.4, bf16[512,2,2,64]{0,3,2,1:T(8,128)(2,1)S(1)} %get-tuple-element.355, bf16[2,2048,2,2,64]{1,4,3,2,0:T(8,128)(2,1)S(1)} %get-tuple-element.354, s32[]{:T(128)S(6)} %copy.38), kind=kOutput, calls=%fused_computation.4.clone.1 | convolution fusion | flops 549451776 | bytes 19144708 | tf_op jit(solution)/shard_map/while/body/eval_jaxpr/qhcd,khcd->hcqk/dot_general | solution.py:120
  98.9 4.2 %select_reduce_fusion.2 = f32[2,2,512]{2,1,0:T(2,128)S(1)} fusion(f32[2,2,2048,512]{3,2,1,0:T(8,128)S(1)} %get-tuple-element.319, f32[2,2,512]{2,1,0:T(2,128)S(1)} %fusion.79, pred[512,2048]{0,1:T(8,128)(4,1)S(1)} %broadcast_compare_fusion.4), kind=kLoop, calls=%fused_computation.3.clone.1 | loop fusion | flops 20969472 | bytes 17842176 | tf_op jit(solution)/shard_map/while/body/eval_jaxpr/reduce_sum | solution.py:136
  103.2 0.6 dynamic_slice.43
  104.5 0.8 broadcast_compare_fusion.4
  105.2 3.0 %fusion.78 = (f32[2,2,512]{2,1,0:T(2,128)S(1)}, f32[2,2,2048,512]{3,2,1,0:T(8,128)S(1)}) fusion(pred[512,2048]{0,1:T(8,128)(4,1)S(1)} %broadcast_compare_fusion.4, bf16[512,2,2,64]{0,3,2,1:T(8,128)(2,1)S(1)} %get-tuple-element.355, bf16[2,2048,2,2,64]{1,4,3,2,0:T(8,128)(2,1)S(1)} %get-tuple-element.354, s32[]{:T(128)S(6)} %copy.38), kind=kOutput, calls=%fused_computation.4.clone.1 | convolution fusion | flops 549451776 | bytes 19144708 | tf_op jit(solution)/shard_map/while/body/eval_jaxpr/qhcd,khcd->hcqk/dot_general | solution.py:120
  108.2 4.2 %select_reduce_fusion.2 = f32[2,2,512]{2,1,0:T(2,128)S(1)} fusion(f32[2,2,2048,512]{3,2,1,0:T(8,128)S(1)} %get-tuple-element.319, f32[2,2,512]{2,1,0:T(2,128)S(1)} %fusion.79, pred[512,2048]{0,1:T(8,128)(4,1)S(1)} %broadcast_compare_fusion.4), kind=kLoop, calls=%fused_computation.3.clone.1 | loop fusion | flops 20969472 | bytes 17842176 | tf_op jit(solution)/shard_map/while/body/eval_jaxpr/reduce_sum | solution.py:136
  112.5 29.0 %all-gather.8.cloned.1.call-done = bf16[4096,2,128]{2,0,1:T(8,128)(2,1)} async-done(((bf16[512,2,128]{2,0,1:T(8,128)(2,1)}), bf16[4096,2,128]{2,0,1:T(8,128)(2,1)}) %all-gather.8.cloned.1.call-update) | async-done | bytes 2097168 | tf_op jit(solution)/shard_map/all_gather | solution.py:163
  141.6 0.0 copy-start.9
  141.6 0.0 copy-start.17
  141.6 23.3 %while.25 = (s32[]{:T(128)}, f32[512,2,128]{0,2,1:T(8,128)}, bf16[2,2048,2,128]{3,1,0,2:T(8,128)(2,1)}, s32[2]{0:T(128)S(1)}, bf16[2,2048,2,2,64]{1,4,3,2,0:T(8,...) while((s32[]{:T(128)}, f32[512,2,128]{0,2,1:T(8,128)}, ...), condition=%wide.region_6.7_spmd.clone, body=%wide.region_5.6_spmd.clone.sunk | while | flops 1102318080 | bytes 51680008 | solution.py:59
  141.6 0.6 dynamic_slice.46
  142.9 0.8 broadcast_compare_fusion.5
  143.6 0.0 copy-start.4
  143.7 7.4 %fusion.85 = f32[2,2,512,2048]{2,3,1,0:T(8,128)S(1)} fusion(f32[2,2,512]{2,1,0:T(2,128)S(1)} %get-tuple-element.393, f32[2,2,512]{2,1,0:T(2,128)S(1)} %get-tuple-element.392, pred[512,2048]{0,1:T(8,128)(4,1)S(1)} %broadcast_compare_fusion.5, bf16[512,2,2,64]{0,3,2,1:T(8,128)(2,1)S(1)} %get-tuple-element.391, ...), kind=kOutput, calls=%fused_computation.20.clone.1 | convolution fusion | flops 557842432 | bytes 19152900 | tf_op jit(solution)/shard_map/while/body/eval_jaxpr/qhcd,khcd->hcqk/dot_general | solution.py:120
  151.1 1.3 fusion.86
  152.4 0.8 copy-done.5
  153.2 0.6 dynamic_slice.46
  154.5 0.8 broadcast_compare_fusion.5
  155.3 0.0 copy-start.4
  155.3 7.4 %fusion.85 = f32[2,2,512,2048]{2,3,1,0:T(8,128)S(1)} fusion(f32[2,2,512]{2,1,0:T(2,128)S(1)} %get-tuple-element.393, f32[2,2,512]{2,1,0:T(2,128)S(1)} %get-tuple-element.392, pred[512,2048]{0,1:T(8,128)(4,1)S(1)} %broadcast_compare_fusion.5, bf16[512,2,2,64]{0,3,2,1:T(8,128)(2,1)S(1)} %get-tuple-element.391, ...), kind=kOutput, calls=%fused_computation.20.clone.1 | convolution fusion | flops 557842432 | bytes 19152900 | tf_op jit(solution)/shard_map/while/body/eval_jaxpr/qhcd,khcd->hcqk/dot_general | solution.py:120
  162.7 1.3 fusion.86
  164.1 0.0 copy-start.5
  164.1 0.8 copy-done.5
  164.9 1.1 multiply_reduce_fusion
  166.0 1.9 multiply_convert_fusion
  167.8 0.0 all-gather.12.cloned.1.call-update
  167.9 0.2 all-gather.14.cloned.1.call-start
  168.2 2.1 %fusion.42 = f32[512,256]{0,1:T(8,128)S(1)} fusion(bf16[2048,256]{1,0:T(8,128)(2,1)} %param.23, bf16[512,2048]{1,0:T(8,128)(2,1)S(1)} %copy-done.2, f32[2048]{0:T(1024)S(1)} %copy-done.17, f32[512]{0:T(512)S(1)} %copy-done.9), kind=kOutput, calls=%fused_computation.58 | convolution fusion | flops 540409856 | bytes 3680256 | tf_op jit(solution)/shard_map/dot_general | solution.py:41
  170.3 0.8 fusion.41
  171.1 0.1 slice.54
  171.2 2.5 %collective-permute-start = (bf16[2,256]{0,1:T(8,128)(2,1)S(1)}, bf16[2,256]{0,1:T(8,128)(2,1)S(1)}, u32[]{:S(2)}, u32[]{:S(2)}) collective-permute-start(bf16[2,256]{0,1:T(8,128)(2,1)S(1)} %slice.54), channel_id=1, source_target_pairs={{0,4},{4,8},{8,12},{12,16},{16,20},{20,24},{24,28},{1,5},{5,9},{9,... | collective-permute-start | bytes 3080 | tf_op jit(solution)/shard_map/ppermute | solution.py:17
  173.7 1.9 collective-permute-done
  175.5 1.6 fusion.45
  177.2 0.0 all-gather.14.cloned.1.call-update
  177.2 0.6 log_add_fusion
  177.8 5.5 %all-gather.12.cloned.1.call-done = bf16[512,1024]{0,1:T(8,128)(2,1)} async-done(((bf16[512,256]{0,1:T(8,128)(2,1)}), bf16[512,1024]{0,1:T(8,128)(2,1)}) %all-gather.12.cloned.1.call-update) | async-done | bytes 1048592 | tf_op jit(solution)/shard_map/all_gather | solution.py:179
  183.3 2.0 fusion.54
  185.2 16.8 %all-gather.14.cloned.1.call-done = bf16[512,1024]{0,1:T(8,128)(2,1)} async-done(((bf16[512,256]{0,1:T(8,128)(2,1)}), bf16[512,1024]{0,1:T(8,128)(2,1)}) %all-gather.14.cloned.1.call-update) | async-done | bytes 1048592 | tf_op jit(solution)/shard_map/all_gather | solution.py:184
  202.0 2.8 %fusion.34 = bf16[512,512]{1,0:T(8,128)(2,1)} fusion(f32[512,512]{1,0:T(8,128)S(1)} %fusion.54, bf16[512,1024]{0,1:T(8,128)(2,1)} %all-gather.14.cloned.1.call-done, bf16[1024,512]{1,0:T(8,128)(2,1)S(1)} %copy-done.15), kind=kOutput, calls=%fused_computation.44 | convolution fusion | flops 537395200 | bytes 3670016 | tf_op jit(solution)/shard_map/dot_general | solution.py:183
  (58 shorter events, 0.3 us)
Async XLA Ops:
  7.2 176.1 %copy-start = (bf16[1024,512]{1,0:T(8,128)(2,1)S(1)}, bf16[1024,512]{1,0:T(8,128)(2,1)}, u32[]{:S(2)}) copy-start(bf16[1024,512]{1,0:T(8,128)(2,1)} %param.28) | copy-start | bytes 3145732
  7.2 32.6 %copy-start.16 = (f32[2048]{0:T(1024)S(1)}, f32[2048]{0:T(1024)}, u32[]{:S(2)}) copy-start(f32[2048]{0:T(1024)} %param.18) | copy-start | bytes 24580
  7.2 27.7 %all-gather.6.cloned.1.call-start = ((), (), s32[]{:S(2)}) async-start(), calls=%async_computation | async-start | bytes 2621440 | tf_op jit(solution)/shard_map/all_gather | solution.py:90
  7.9 84.1 %all-gather.10.cloned.1.call-start = ((), (), s32[]{:S(2)}) async-start(), calls=%async_computation.2 | async-start | bytes 2359296 | tf_op jit(solution)/shard_map/all_gather | solution.py:162
  34.9 4.9 %copy-start.1 = (bf16[512,2048]{1,0:T(8,128)(2,1)S(1)}, bf16[512,2048]{1,0:T(8,128)(2,1)}, u32[]{:S(2)}) copy-start(bf16[512,2048]{1,0:T(8,128)(2,1)} %all-gather.6.cloned.1.call-done) | copy-start | bytes 6291460
  34.9 4.9 %copy-start.12 = (bf16[2048,256]{1,0:T(8,128)(2,1)S(1)}, bf16[2048,256]{1,0:T(8,128)(2,1)}, u32[]{:S(2)}) copy-start(bf16[2048,256]{1,0:T(8,128)(2,1)} %param.19) | copy-start | bytes 3145732
  37.1 4.5 %copy-start.8 = (f32[512]{0:T(512)}, f32[512]{0:T(512)S(1)}, u32[]{:S(2)}) copy-start(f32[512]{0:T(512)S(1)} %add_rsqrt_fusion.1) | copy-start | bytes 6148
  41.5 100.0 %all-gather.8.cloned.1.call-start = ((), (), s32[]{:S(2)}) async-start(), calls=%async_computation.1 | async-start | bytes 2359296 | tf_op jit(solution)/shard_map/all_gather | solution.py:163
  46.1 137.1 %all-gather.12.cloned.1.call-start = ((), (), s32[]{:S(2)}) async-start(), calls=%async_computation.3 | async-start | bytes 1310720 | tf_op jit(solution)/shard_map/all_gather | solution.py:179
  46.9 46.9 %copy-start.6 = (bf16[512,2,2,64]{0,3,2,1:T(8,128)(2,1)S(1)}, bf16[512,2,2,64]{0,3,2,1:T(8,128)(2,1)}, u32[]{:S(2)}) copy-start(bf16[512,2,2,64]{0,3,2,1:T(8,128)(2,1)} %pad_maximum_fusion.2) | copy-start | bytes 786436
  93.8 47.7 %copy-start.18 = (f32[2]{0:T(128)S(1)}, f32[2]{0:T(128)}, u32[]{:S(2)}) copy-start(f32[2]{0:T(128)} %param.26) | copy-start | bytes 28
  112.5 29.1 %copy-start.3 = (bf16[2,2048,2,2,64]{1,4,3,2,0:T(8,128)(2,1)}, bf16[2,2048,2,2,64]{1,4,3,2,0:T(8,128)(2,1)S(1)}, u32[]{:S(2)}) copy-start(bf16[2,2048,2,2,64]{1,4,3,2,0:T(8,128)(2,1)S(1)} %get-tuple-element.405) | copy-start | bytes 6291460
  141.5 24.4 %copy-start.10 = (f32[128]{0:T(128)S(1)}, f32[128]{0:T(128)}, u32[]{:S(2)}) copy-start(f32[128]{0:T(128)} %param.27) | copy-start | bytes 1540
  141.5 26.6 %copy-start.2 = (bf16[512,2048]{1,0:T(8,128)(2,1)S(1)}, bf16[512,2048]{1,0:T(8,128)(2,1)}, u32[]{:S(2)}) copy-start(bf16[512,2048]{1,0:T(8,128)(2,1)} %all-gather.6.cloned.1.call-done) | copy-start | bytes 6291460
  141.6 26.6 %copy-start.9 = (f32[512]{0:T(512)S(1)}, f32[512]{0:T(512)}, u32[]{:S(2)}) copy-start(f32[512]{0:T(512)} %copy-done.8) | copy-start | bytes 6148
  141.6 26.6 %copy-start.17 = (f32[2048]{0:T(1024)S(1)}, f32[2048]{0:T(1024)}, u32[]{:S(2)}) copy-start(f32[2048]{0:T(1024)} %param.18) | copy-start | bytes 24580
  143.6 7.5 %copy-start.4 = (f32[512,2,128]{0,2,1:T(8,128)S(1)}, f32[512,2,128]{0,2,1:T(8,128)}, u32[]{:S(2)}) copy-start(f32[512,2,128]{0,2,1:T(8,128)} %get-tuple-element.374) | copy-start | bytes 1572868 | tf_op jit(solution)/shard_map/while
  143.7 7.5 %copy-start.11 = (bf16[2,2048,2,128]{3,1,0,2:T(8,128)(2,1)S(1)}, bf16[2,2048,2,128]{3,1,0,2:T(8,128)(2,1)}, u32[]{:S(2)}) copy-start(bf16[2,2048,2,128]{3,1,0,2:T(8,128)(2,1)} %get-tuple-element.388) | copy-start | bytes 6291460 | tf_op jit(solution)/shard_map/while
  152.4 0.8 copy-start.5
  155.3 7.4 %copy-start.4 = (f32[512,2,128]{0,2,1:T(8,128)S(1)}, f32[512,2,128]{0,2,1:T(8,128)}, u32[]{:S(2)}) copy-start(f32[512,2,128]{0,2,1:T(8,128)} %get-tuple-element.374) | copy-start | bytes 1572868 | tf_op jit(solution)/shard_map/while
  155.3 7.4 %copy-start.11 = (bf16[2,2048,2,128]{3,1,0,2:T(8,128)(2,1)S(1)}, bf16[2,2048,2,128]{3,1,0,2:T(8,128)(2,1)}, u32[]{:S(2)}) copy-start(bf16[2,2048,2,128]{3,1,0,2:T(8,128)(2,1)} %get-tuple-element.388) | copy-start | bytes 6291460 | tf_op jit(solution)/shard_map/while
  164.1 0.8 copy-start.5
  167.9 5.8 %copy-start.7 = (f32[3,256]{1,0:T(4,128)S(1)}, f32[3,256]{1,0:T(4,128)}, u32[]{:S(2)}) copy-start(f32[3,256]{1,0:T(4,128)} %param.25) | copy-start | bytes 9220
  167.9 34.1 %all-gather.14.cloned.1.call-start = ((), (), s32[]{:S(2)}) async-start(), calls=%async_computation.4 | async-start | bytes 1310720 | tf_op jit(solution)/shard_map/all_gather | solution.py:184
  168.1 2.2 %copy-start.13 = (bf16[2048,256]{1,0:T(8,128)(2,1)S(1)}, bf16[2048,256]{1,0:T(8,128)(2,1)}, u32[]{:S(2)}) copy-start(bf16[2048,256]{1,0:T(8,128)(2,1)} %param.24) | copy-start | bytes 3145732
  168.2 7.4 %copy-start.14 = (bf16[2048,256]{1,0:T(8,128)(2,1)S(1)}, bf16[2048,256]{1,0:T(8,128)(2,1)}, u32[]{:S(2)}) copy-start(bf16[2048,256]{1,0:T(8,128)(2,1)} %param.22) | copy-start | bytes 3145732
  171.2 4.3 %collective-permute-start = (bf16[2,256]{0,1:T(8,128)(2,1)S(1)}, bf16[2,256]{0,1:T(8,128)(2,1)S(1)}, u32[]{:S(2)}, u32[]{:S(2)}) collective-permute-start(bf16[2,256]{0,1:T(8,128)(2,1)S(1)} %slice.54), channel_id=1, source_target_pairs={{0,4},{4,8},{8,12},{12,16},{16,20},{20,24},{24,28},{1,5},{5,9},{9,... | collective-permute-start | bytes 3080 | tf_op jit(solution)/shard_map/ppermute | solution.py:17
  177.2 24.8 %copy-start.15 = (bf16[1024,512]{1,0:T(8,128)(2,1)S(1)}, bf16[1024,512]{1,0:T(8,128)(2,1)}, u32[]{:S(2)}) copy-start(bf16[1024,512]{1,0:T(8,128)(2,1)} %param.29) | copy-start | bytes 3145732
Sparse Core Ops, SparseCore 0:
  9.6 25.2 all-gather.5
  41.6 50.3 all-gather.9
  94.2 47.2 all-gather.7
  168.0 15.2 all-gather.11
  185.2 16.6 all-gather.13
where the time goes:
time: 212 us; the launch traced here: 211 us
  waiting for transfers between devices  126 us (59%)
  matrix products  38.8 us (18%)
  other arithmetic  19.3 us (9%)
  between operations  14.1 us (7%)
  local copies, waits for them, and re-layouts  7.83 us (4%)
  starting transfers between devices  2.84 us (1%)
  loops' own time  2.83 us (1%)
    all_gather x1, waiting for transfers between devices, per_device(): lax.all_gather(key_rows, 'sp', axis=0, tiled=True)  45.2 us
    all_gather x1, waiting for transfers between devices, per_device(): lax.all_gather(values, 'sp', axis=0, tiled=True)  29 us
    all_gather x1, waiting for transfers between devices, per_device(): lax.all_gather(tokens, 'tp', axis=1, tiled=True)  26.6 us
    dot_general x4, matrix products, block_scores(): jnp.einsum('qhcd,khcd->hcqk', queries, key_block, preferred_element_type=...  20.8 us
    all_gather x1, waiting for transfers between devices, per_device(): lax.all_gather(conv_out, 'tp', axis=1, tiled=True)  16.8 us
    dot_general x6, matrix products, add_products(): jnp.dot(scaled, weight, preferred_element_type=jnp.float32)  10.6 us
    reduce_sum x2, other arithmetic, stats_step(): jnp.sum(exponent, axis=-1)  8.38 us
    all_gather x1, waiting for transfers between devices, per_device(): lax.all_gather(attn_out, 'tp', axis=1, tiled=True)  5.45 us
  transfers between devices with their start and end apart: 6, of which 6 were waited for; matrix products, arithmetic and copies ran while one was open for 15% of the time, Pallas kernels for 0%

commit v1 on v0

--- a/solution.py
+++ b/solution.py
@@ -3,6 +3,7 @@
 import jax.numpy as jnp
 from jax import lax
 from jax.sharding import PartitionSpec as P
+from jax.lax import all_gather
 
 NORM_EPS = 1e-06
 HEAD_EPS = 1e-05
@@ -77,6 +78,11 @@
     attn_out_weight,
     conv_out_weight,
 ):
+
+    def settle_vectors(chunk, chip_axis):
+        base_arr = jnp.concatenate(all_gather(chunk, axis_name=chip_axis), axis=1)
+        return base_arr
+
     local_rows = tokens.shape[0]
     local_heads = lambdas.shape[0]
     head_dim = query_weight.shape[1] // (2 * local_heads)
@@ -181,9 +187,7 @@
         preferred_element_type=jnp.float32,
     )
     mixed_out = running + jnp.dot(
-        lax.all_gather(conv_out, "tp", axis=1, tiled=True),
-        conv_out_weight,
-        preferred_element_type=jnp.float32,
+        settle_vectors(conv_out, "tp"), conv_out_weight, preferred_element_type=jnp.float32
     )
     return (mixed_out.astype(jnp.bfloat16), log_totals)
 

time: 212 us -> 190 us (0.90)
  waiting for transfers between devices: 126 us -> 106 us
  matrix products: 38.8 us -> 34.3 us
    all_gather x1, waiting for transfers between devices: 16.8 us -> 0.02 us  [settle_vectors(): base_arr = jnp.concatenate(all_gather(chunk, axis_name=chip_axis), axis=1)]
    all_gather x1, waiting for transfers between devices: 45.2 us -> 35 us  [per_device(): lax.all_gather(key_rows, 'sp', axis=0, tiled=True)]
    all_gather x1, waiting for transfers between devices: 5.45 us -> 13.4 us  [per_device(): lax.all_gather(attn_out, 'tp', axis=1, tiled=True)]
    dot_general x4, matrix products: 20.8 us -> 17.6 us  [block_scores(): jnp.einsum('qhcd,khcd->hcqk', queries, key_block, preferred_element_type=...]
  transfers between devices with their start and end apart: 6 -> 6, of which waited for: 6 -> 5; matrix products, arithmetic and copies ran while one was open for 15% -> 27% of each run, Pallas kernels for 0% -> 0%
where the time goes in v1:
time: 190 us
  waiting for transfers between devices  106 us (56%)
  matrix products  34.3 us (18%)
  other arithmetic  19.4 us (10%)
  between operations  14.1 us (7%)
  local copies, waits for them, and re-layouts  9.77 us (5%)
  starting transfers between devices  3.58 us (2%)
  loops' own time  3.07 us (2%)
    all_gather x1, waiting for transfers between devices, per_device(): lax.all_gather(key_rows, 'sp', axis=0, tiled=True)  35 us
    all_gather x1, waiting for transfers between devices, per_device(): lax.all_gather(values, 'sp', axis=0, tiled=True)  28.9 us
    all_gather x1, waiting for transfers between devices, per_device(): lax.all_gather(tokens, 'tp', axis=1, tiled=True)  26.6 us
    dot_general x4, matrix products, block_scores(): jnp.einsum('qhcd,khcd->hcqk', queries, key_block, preferred_element_type=...  17.6 us
    all_gather x1, waiting for transfers between devices, per_device(): lax.all_gather(attn_out, 'tp', axis=1, tiled=True)  13.4 us
    dot_general x6, matrix products, add_products(): jnp.dot(scaled, weight, preferred_element_type=jnp.float32)  10.6 us
    reduce_sum x2, other arithmetic, stats_step(): jnp.sum(exponent, axis=-1)  8.38 us
  transfers between devices with their start and end apart: 6, of which 5 were waited for; matrix products, arithmetic and copies ran while one was open for 27% of the time, Pallas kernels for 0%

profile of v1, /device:TPU:0, one launch (start us, length us, event | category | flops | bytes accessed | tf_op | source)
XLA Modules:
  0.0 190.0 jit_solution(15616992371786437364)
XLA Ops:
  7.2 0.0 copy-start
  7.2 0.0 copy-start.13
  7.2 0.0 all-gather.7.cloned.1.call-start
  7.2 0.7 all-gather.7.cloned.1.call-update
  7.9 0.0 all-gather.11.cloned.1.call-start
  8.0 0.3 multiply_cosine_fusion
  8.3 26.6 %all-gather.7.cloned.1.call-done = bf16[512,2048]{1,0:T(8,128)(2,1)} async-done(((bf16[512,512]{1,0:T(8,128)(2,1)}), bf16[512,2048]{1,0:T(8,128)(2,1)}) %all-gather.7.cloned.1.call-update) | async-done | bytes 2097168 | tf_op jit(solution)/shard_map/all_gather | solution.py:96
  34.9 2.2 %fusion.32 = f32[512]{0:T(512)S(1)} fusion(bf16[512,2048]{1,0:T(8,128)(2,1)} %all-gather.7.cloned.1.call-done), kind=kLoop, calls=%fused_computation.40 | loop fusion | flops 3145216 | bytes 2099200 | tf_op jit(solution)/shard_map/reduce_sum | solution.py:44
  37.1 2.6 %convolution_multiply_fusion.4 = f32[512,256]{0,1:T(8,128)S(1)} fusion(bf16[2048,256]{1,0:T(8,128)(2,1)} %param.20, bf16[512,2048]{1,0:T(8,128)(2,1)} %all-gather.7.cloned.1.call-done, f32[2048]{0:T(1024)} %param.18, f32[512]{0:T(512)S(1)} %add_rsqrt_fusion.1), kind=kOutput, calls=%fused_computation.49 | convolution fusion | flops 540147712 | bytes 3680256 | tf_op jit(solution)/shard_map/dot_general | solution.py:42
  39.8 0.8 convolution_multiply_fusion.3
  40.6 0.2 subtract_convert_fusion
  40.8 0.7 pad_maximum_fusion.1
  41.5 0.0 all-gather.11.cloned.1.call-update
  41.5 0.0 copy-start.14
  41.5 0.0 all-gather.9.cloned.1.call-start
  41.6 2.7 %fusion.35 = bf16[512,256]{0,1:T(8,128)(2,1)} fusion(bf16[2048,256]{1,0:T(8,128)(2,1)} %param.21, bf16[512,2048]{1,0:T(8,128)(2,1)S(1)} %copy-done.1, f32[2048]{0:T(1024)S(1)} %copy-done.13, f32[512]{0:T(512)S(1)} %add_rsqrt_fusion.1), kind=kOutput, calls=%fused_computation.51 | convolution fusion | flops 540278784 | bytes 3418112 | tf_op jit(solution)/shard_map/dot_general | solution.py:42
  44.3 1.8 copy.22
  46.1 0.0 all-gather.9.cloned.1.call-update
  46.1 0.0 all-gather.15.cloned.1.call-start
  46.2 0.8 fusion.53
  47.0 2.1 %fusion.42 = f32[512,256]{0,1:T(8,128)S(1)} fusion(bf16[2048,256]{1,0:T(8,128)(2,1)} %param.23, bf16[512,2048]{1,0:T(8,128)(2,1)S(1)} %copy-done.1, f32[2048]{0:T(1024)} %param.18, f32[512]{0:T(512)} %copy-done.5), kind=kOutput, calls=%fused_computation.58 | convolution fusion | flops 540409856 | bytes 3680256 | tf_op jit(solution)/shard_map/dot_general | solution.py:42
  49.1 0.8 fusion.41
  49.9 0.1 slice.54
  50.0 3.4 %collective-permute-start = (bf16[2,256]{0,1:T(8,128)(2,1)S(1)}, bf16[2,256]{0,1:T(8,128)(2,1)S(1)}, u32[]{:S(2)}, u32[]{:S(2)}) collective-permute-start(bf16[2,256]{0,1:T(8,128)(2,1)S(1)} %slice.54), channel_id=1, source_target_pairs={{0,4},{4,8},{8,12},{12,16},{16,20},{20,24},{24,28},{1,5},{5,9},{9,... | collective-permute-start | bytes 3080 | tf_op jit(solution)/shard_map/ppermute | solution.py:18
  53.4 0.7 pad_maximum_fusion.2
  54.1 1.2 collective-permute-done
  55.3 1.6 fusion.45
  56.9 0.0 all-gather.15.cloned.1.call-update
  56.9 0.0 all-gather.13.cloned.1.call-start
  57.0 35.0 %all-gather.11.cloned.1.call-done = bf16[4096,2,2,64]{0,3,2,1:T(8,128)(2,1)} async-done(((bf16[512,2,2,64]{0,3,2,1:T(8,128)(2,1)}), bf16[4096,2,2,64]{0,3,2,1:T(8,128)(2,1)}) %all-gather.11.cloned.1.call-update) | async-done | bytes 2097168 | tf_op jit(solution)/shard_map/all_gather | solution.py:168
  92.0 1.7 copy.40
  93.7 0.0 copy-start.15
  93.7 18.8 %while.24 = (s32[]{:T(128)}, f32[2,2,512]{2,1,0:T(2,128)S(1)}, f32[2,2,512]{2,1,0:T(2,128)S(1)}, s32[2]{0:T(128)S(1)}, bf16[2,2048,2,2,64]{1,4,3,2,0:T(8,128)(2,...) while((s32[]{:T(128)}, f32[2,2,512]{2,1,0:T(2,128)S(1)}, ...), condition=%wide.region_4.5_spmd.clone, body=%wide.region_1.4_spmd.clone.sunk | while | flops 571486720 | bytes 38138008 | solution.py:60
  93.9 0.6 dynamic_slice.43
  95.2 0.8 broadcast_compare_fusion.4
  96.0 3.0 %fusion.78 = (f32[2,2,512]{2,1,0:T(2,128)S(1)}, f32[2,2,2048,512]{3,2,1,0:T(8,128)S(1)}) fusion(pred[512,2048]{0,1:T(8,128)(4,1)S(1)} %broadcast_compare_fusion.4, bf16[512,2,2,64]{0,3,2,1:T(8,128)(2,1)S(1)} %get-tuple-element.355, bf16[2,2048,2,2,64]{1,4,3,2,0:T(8,128)(2,1)S(1)} %get-tuple-element.354, s32[]{:T(128)S(6)} %copy.45), kind=kOutput, calls=%fused_computation.4.clone.1 | convolution fusion | flops 549451776 | bytes 19144708 | tf_op jit(solution)/shard_map/while/body/eval_jaxpr/qhcd,khcd->hcqk/dot_general | solution.py:126
  99.0 4.2 %select_reduce_fusion.2 = f32[2,2,512]{2,1,0:T(2,128)S(1)} fusion(f32[2,2,2048,512]{3,2,1,0:T(8,128)S(1)} %get-tuple-element.319, f32[2,2,512]{2,1,0:T(2,128)S(1)} %fusion.79, pred[512,2048]{0,1:T(8,128)(4,1)S(1)} %broadcast_compare_fusion.4), kind=kLoop, calls=%fused_computation.3.clone.1 | loop fusion | flops 20969472 | bytes 17842176 | tf_op jit(solution)/shard_map/while/body/eval_jaxpr/reduce_sum | solution.py:142
  103.2 0.6 dynamic_slice.43
  104.5 0.8 broadcast_compare_fusion.4
  105.3 3.0 %fusion.78 = (f32[2,2,512]{2,1,0:T(2,128)S(1)}, f32[2,2,2048,512]{3,2,1,0:T(8,128)S(1)}) fusion(pred[512,2048]{0,1:T(8,128)(4,1)S(1)} %broadcast_compare_fusion.4, bf16[512,2,2,64]{0,3,2,1:T(8,128)(2,1)S(1)} %get-tuple-element.355, bf16[2,2048,2,2,64]{1,4,3,2,0:T(8,128)(2,1)S(1)} %get-tuple-element.354, s32[]{:T(128)S(6)} %copy.45), kind=kOutput, calls=%fused_computation.4.clone.1 | convolution fusion | flops 549451776 | bytes 19144708 | tf_op jit(solution)/shard_map/while/body/eval_jaxpr/qhcd,khcd->hcqk/dot_general | solution.py:126
  108.3 4.2 %select_reduce_fusion.2 = f32[2,2,512]{2,1,0:T(2,128)S(1)} fusion(f32[2,2,2048,512]{3,2,1,0:T(8,128)S(1)} %get-tuple-element.319, f32[2,2,512]{2,1,0:T(2,128)S(1)} %fusion.79, pred[512,2048]{0,1:T(8,128)(4,1)S(1)} %broadcast_compare_fusion.4), kind=kLoop, calls=%fused_computation.3.clone.1 | loop fusion | flops 20969472 | bytes 17842176 | tf_op jit(solution)/shard_map/while/body/eval_jaxpr/reduce_sum | solution.py:142
  112.5 28.9 %all-gather.9.cloned.1.call-done = bf16[4096,2,128]{2,0,1:T(8,128)(2,1)} async-done(((bf16[512,2,128]{2,0,1:T(8,128)(2,1)}), bf16[4096,2,128]{2,0,1:T(8,128)(2,1)}) %all-gather.9.cloned.1.call-update) | async-done | bytes 2097168 | tf_op jit(solution)/shard_map/all_gather | solution.py:169
  141.5 20.0 %while.25 = (s32[]{:T(128)}, f32[512,2,128]{0,2,1:T(8,128)}, bf16[2,2048,2,128]{3,1,0,2:T(8,128)(2,1)}, s32[2]{0:T(128)S(1)}, bf16[2,2048,2,2,64]{1,4,3,2,0:T(8,...) while((s32[]{:T(128)}, f32[512,2,128]{0,2,1:T(8,128)}, ...), condition=%wide.region_6.7_spmd.clone, body=%wide.region_5.6_spmd.clone.sunk | while | flops 1102318080 | bytes 51680008 | solution.py:60
  141.5 0.6 dynamic_slice.46
  142.7 0.8 broadcast_compare_fusion.5
  143.5 0.0 copy-start.2
  143.5 5.8 %fusion.85 = f32[2,2,512,2048]{2,3,1,0:T(8,128)S(1)} fusion(f32[2,2,512]{2,1,0:T(2,128)S(1)} %get-tuple-element.393, f32[2,2,512]{2,1,0:T(2,128)S(1)} %get-tuple-element.392, pred[512,2048]{0,1:T(8,128)(4,1)S(1)} %broadcast_compare_fusion.5, bf16[512,2,2,64]{0,3,2,1:T(8,128)(2,1)S(1)} %get-tuple-element.391, ...), kind=kOutput, calls=%fused_computation.20.clone.1 | convolution fusion | flops 557842432 | bytes 19152900 | tf_op jit(solution)/shard_map/while/body/eval_jaxpr/qhcd,khcd->hcqk/dot_general | solution.py:126
  149.4 1.3 fusion.86
  150.7 0.0 copy-start.3
  150.7 0.8 copy-done.3
  151.5 0.6 dynamic_slice.46
  152.7 0.8 broadcast_compare_fusion.5
  153.5 5.8 %fusion.85 = f32[2,2,512,2048]{2,3,1,0:T(8,128)S(1)} fusion(f32[2,2,512]{2,1,0:T(2,128)S(1)} %get-tuple-element.393, f32[2,2,512]{2,1,0:T(2,128)S(1)} %get-tuple-element.392, pred[512,2048]{0,1:T(8,128)(4,1)S(1)} %broadcast_compare_fusion.5, bf16[512,2,2,64]{0,3,2,1:T(8,128)(2,1)S(1)} %get-tuple-element.391, ...), kind=kOutput, calls=%fused_computation.20.clone.1 | convolution fusion | flops 557842432 | bytes 19152900 | tf_op jit(solution)/shard_map/while/body/eval_jaxpr/qhcd,khcd->hcqk/dot_general | solution.py:126
  159.4 1.3 fusion.86
  160.7 0.8 copy-done.3
  161.5 1.1 multiply_reduce_fusion
  162.6 2.0 %multiply_convert_fusion = bf16[512,2,128]{0,2,1:T(8,128)(2,1)} fusion(f32[512,2,128]{0,2,1:T(8,128)} %get-tuple-element.94, f32[128]{0:T(128)S(1)} %copy-done.7, f32[512,2]{0,1:T(2,128)S(1)} %add_rsqrt_fusion), kind=kLoop, calls=%fused_computation.63 | loop fusion | flops 524288 | bytes 791040 | tf_op jit(solution)/shard_map/convert_element_type | solution.py:182
  164.6 0.0 all-gather.13.cloned.1.call-update
  164.6 0.0 all-gather.15.cloned.1.call-done
  164.6 1.3 copy.41
  165.9 0.6 log_add_fusion
  166.6 13.4 %all-gather.13.cloned.1.call-done = bf16[512,1024]{0,1:T(8,128)(2,1)} async-done(((bf16[512,256]{0,1:T(8,128)(2,1)}), bf16[512,1024]{0,1:T(8,128)(2,1)}) %all-gather.13.cloned.1.call-update) | async-done | bytes 1048592 | tf_op jit(solution)/shard_map/all_gather | solution.py:185
  180.0 2.0 %fusion.54 = f32[512,512]{1,0:T(8,128)S(1)} fusion(bf16[512,1024]{0,1:T(8,128)(2,1)} %all-gather.13.cloned.1.call-done, bf16[1024,512]{1,0:T(8,128)(2,1)S(1)} %copy-done), kind=kOutput, calls=%fused_computation.83 | convolution fusion | flops 536870912 | bytes 3145728 | tf_op jit(solution)/shard_map/dot_general | solution.py:184
  181.9 1.5 fusion.34
  (53 shorter events, 0.2 us)
Async XLA Ops:
  7.2 172.8 %copy-start = (bf16[1024,512]{1,0:T(8,128)(2,1)S(1)}, bf16[1024,512]{1,0:T(8,128)(2,1)}, u32[]{:S(2)}) copy-start(bf16[1024,512]{1,0:T(8,128)(2,1)} %param.28) | copy-start | bytes 3145732
  7.2 32.6 %copy-start.13 = (f32[2048]{0:T(1024)S(1)}, f32[2048]{0:T(1024)}, u32[]{:S(2)}) copy-start(f32[2048]{0:T(1024)} %param.18) | copy-start | bytes 24580
  7.2 27.7 %all-gather.7.cloned.1.call-start = ((), (), s32[]{:S(2)}) async-start(), calls=%async_computation | async-start | bytes 2621440 | tf_op jit(solution)/shard_map/all_gather | solution.py:96
  7.9 84.0 %all-gather.11.cloned.1.call-start = ((), (), s32[]{:S(2)}) async-start(), calls=%async_computation.2 | async-start | bytes 2359296 | tf_op jit(solution)/shard_map/all_gather | solution.py:168
  34.9 4.9 %copy-start.1 = (bf16[512,2048]{1,0:T(8,128)(2,1)S(1)}, bf16[512,2048]{1,0:T(8,128)(2,1)}, u32[]{:S(2)}) copy-start(bf16[512,2048]{1,0:T(8,128)(2,1)} %all-gather.7.cloned.1.call-done) | copy-start | bytes 6291460
  34.9 4.9 %copy-start.9 = (bf16[2048,256]{1,0:T(8,128)(2,1)S(1)}, bf16[2048,256]{1,0:T(8,128)(2,1)}, u32[]{:S(2)}) copy-start(bf16[2048,256]{1,0:T(8,128)(2,1)} %param.19) | copy-start | bytes 3145732
  37.1 4.5 %copy-start.5 = (f32[512]{0:T(512)}, f32[512]{0:T(512)S(1)}, u32[]{:S(2)}) copy-start(f32[512]{0:T(512)S(1)} %add_rsqrt_fusion.1) | copy-start | bytes 6148
  41.5 7.6 %copy-start.14 = (f32[2048]{0:T(1024)S(1)}, f32[2048]{0:T(1024)}, u32[]{:S(2)}) copy-start(f32[2048]{0:T(1024)} %param.18) | copy-start | bytes 24580
  41.5 99.9 %all-gather.9.cloned.1.call-start = ((), (), s32[]{:S(2)}) async-start(), calls=%async_computation.1 | async-start | bytes 2359296 | tf_op jit(solution)/shard_map/all_gather | solution.py:169
  44.3 4.8 %copy-start.6 = (f32[512]{0:T(512)S(1)}, f32[512]{0:T(512)}, u32[]{:S(2)}) copy-start(f32[512]{0:T(512)} %copy-done.5) | copy-start | bytes 6148
  46.1 118.5 %all-gather.15.cloned.1.call-start = ((), (), s32[]{:S(2)}) async-start(), calls=%async_computation.4 | async-start | bytes 1310720 | tf_op jit(solution)/shard_map/all_gather | solution.py:83
  46.2 2.9 %copy-start.10 = (bf16[2048,256]{1,0:T(8,128)(2,1)S(1)}, bf16[2048,256]{1,0:T(8,128)(2,1)}, u32[]{:S(2)}) copy-start(bf16[2048,256]{1,0:T(8,128)(2,1)} %param.24) | copy-start | bytes 3145732
  47.0 8.3 %copy-start.11 = (bf16[2048,256]{1,0:T(8,128)(2,1)S(1)}, bf16[2048,256]{1,0:T(8,128)(2,1)}, u32[]{:S(2)}) copy-start(bf16[2048,256]{1,0:T(8,128)(2,1)} %param.22) | copy-start | bytes 3145732
  50.0 5.3 %collective-permute-start = (bf16[2,256]{0,1:T(8,128)(2,1)S(1)}, bf16[2,256]{0,1:T(8,128)(2,1)S(1)}, u32[]{:S(2)}, u32[]{:S(2)}) collective-permute-start(bf16[2,256]{0,1:T(8,128)(2,1)S(1)} %slice.54), channel_id=1, source_target_pairs={{0,4},{4,8},{8,12},{12,16},{16,20},{20,24},{24,28},{1,5},{5,9},{9,... | collective-permute-start | bytes 3080 | tf_op jit(solution)/shard_map/ppermute | solution.py:18
  55.3 38.4 %copy-start.4 = (bf16[512,2,2,64]{0,3,2,1:T(8,128)(2,1)S(1)}, bf16[512,2,2,64]{0,3,2,1:T(8,128)(2,1)}, u32[]{:S(2)}) copy-start(bf16[512,2,2,64]{0,3,2,1:T(8,128)(2,1)} %pad_maximum_fusion.2) | copy-start | bytes 786436
  56.9 123.0 %all-gather.13.cloned.1.call-start = ((), (), s32[]{:S(2)}) async-start(), calls=%async_computation.3 | async-start | bytes 1310720 | tf_op jit(solution)/shard_map/all_gather | solution.py:185
  93.7 47.7 %copy-start.15 = (f32[2]{0:T(128)S(1)}, f32[2]{0:T(128)}, u32[]{:S(2)}) copy-start(f32[2]{0:T(128)} %param.26) | copy-start | bytes 28
  141.4 21.1 %copy-start.7 = (f32[128]{0:T(128)S(1)}, f32[128]{0:T(128)}, u32[]{:S(2)}) copy-start(f32[128]{0:T(128)} %param.27) | copy-start | bytes 1540
  143.5 5.9 %copy-start.2 = (f32[512,2,128]{0,2,1:T(8,128)S(1)}, f32[512,2,128]{0,2,1:T(8,128)}, u32[]{:S(2)}) copy-start(f32[512,2,128]{0,2,1:T(8,128)} %get-tuple-element.374) | copy-start | bytes 1572868 | tf_op jit(solution)/shard_map/while
  143.5 5.9 %copy-start.8 = (bf16[2,2048,2,128]{3,1,0,2:T(8,128)(2,1)S(1)}, bf16[2,2048,2,128]{3,1,0,2:T(8,128)(2,1)}, u32[]{:S(2)}) copy-start(bf16[2,2048,2,128]{3,1,0,2:T(8,128)(2,1)} %get-tuple-element.388) | copy-start | bytes 6291460 | tf_op jit(solution)/shard_map/while
  150.7 0.8 copy-start.3
  153.5 5.9 %copy-start.2 = (f32[512,2,128]{0,2,1:T(8,128)S(1)}, f32[512,2,128]{0,2,1:T(8,128)}, u32[]{:S(2)}) copy-start(f32[512,2,128]{0,2,1:T(8,128)} %get-tuple-element.374) | copy-start | bytes 1572868 | tf_op jit(solution)/shard_map/while
  153.5 5.9 %copy-start.8 = (bf16[2,2048,2,128]{3,1,0,2:T(8,128)(2,1)S(1)}, bf16[2,2048,2,128]{3,1,0,2:T(8,128)(2,1)}, u32[]{:S(2)}) copy-start(bf16[2,2048,2,128]{3,1,0,2:T(8,128)(2,1)} %get-tuple-element.388) | copy-start | bytes 6291460 | tf_op jit(solution)/shard_map/while
  160.7 0.8 copy-start.3
  162.6 19.3 %copy-start.12 = (bf16[1024,512]{1,0:T(8,128)(2,1)S(1)}, bf16[1024,512]{1,0:T(8,128)(2,1)}, u32[]{:S(2)}) copy-start(bf16[1024,512]{1,0:T(8,128)(2,1)} %param.29) | copy-start | bytes 3145732
Sparse Core Ops, SparseCore 0:
  9.6 25.2 all-gather.6
  41.6 50.2 all-gather.10
  94.2 47.2 all-gather.8
  142.9 15.2 all-gather.14
  164.7 15.2 all-gather.12
